TPU v7x, 32 devices: a whole 2x2x4 slice. The times are simulated.
32 devices in a mesh: grp: 2 (over y), sp: 4 (over z), tp: 4 (over x, core).
Axes of the slice: x: 2, y: 2, z: 4, core: 2. Of those that a mesh axis runs over, the one named last changes fastest.
Arguments:
- tokens: bfloat16 [3072, 2048], P(('grp', 'sp'), 'tp'), parts along dimension 0, may hold values from -6 to 6
- norm_gain: float32 [2048], replicated, may hold values from 0.1 to 1.9
- qk_gain: float32 [4, 64], replicated, may hold values from 0.7 to 5.5
- w_query_window: bfloat16 [2048, 1024], P('sp', 'tp'), may hold values from -1 to 1
- w_key_window: bfloat16 [2048, 512], P('sp', 'tp'), may hold values from -1 to 1
- w_value_window: bfloat16 [2048, 512], P('sp', 'tp'), may hold values from -0.125 to 0.125
- sink_logits: float32 [16], P('tp'), may hold values from 0 to 5
- w_query_forget: bfloat16 [2048, 1024], P('sp', 'tp'), may hold values from -1 to 1
- w_key_forget: bfloat16 [2048, 1024], P('sp', 'tp'), may hold values from -1 to 1
- w_value_forget: bfloat16 [2048, 1024], P('sp', 'tp'), may hold values from -0.125 to 0.125
- gate_cum: float32 [3072, 16], P(('grp', 'sp'), 'tp'), parts along dimension 0, as said below
- w_merge: bfloat16 [2048, 2, 2048], P('sp', None, 'tp'), may hold values from -0.125 to 0.125
- w_branch: bfloat16 [2, 1024, 2048], P(None, 'sp', 'tp'), may hold values from -0.8984375 to 0.8984375
Outputs:
- mixed: bfloat16 [3072, 2048], P(('grp', 'sp'), 'tp'), parts along dimension 0
There are 2 independent parts, one for each index of `grp`. A program takes and returns all parts, laid end to end along the dimension named above; an argument that names none is the same for every part. Nothing has to cross between parts.
Inputs may be any that keep to these rules, and one draw needn't show every extreme that they name: `gate_cum`: along positions each head's values never rise.
All inputs are finite; a program needn't handle non-finite values.
Results may differ from a plain program's by a relative error of at most 0.012.
Values may be sent and summed in bfloat16 or wider, within the bound.
A program may use at most 64 MiB of HBM per device.

v0:
```python
import math
import jax
import jax.numpy as jnp
from jax import lax
from jax.sharding import PartitionSpec as P

HEAD = 64
WINDOW = 128
epsilon = 1e-06
big_negative = -1e30


def from_behind(value, axis, by):
    size = lax.axis_size(axis)
    pairs = [(i, i + by) for i in range(size) if 0 <= i + by < size]
    return lax.ppermute(value, axis, pairs)


def head_norm(raw, gain, head_count):
    split = raw.reshape(raw.shape[0], head_count, -1)
    scaled = split * lax.rsqrt(jnp.mean(split * split, axis=-1, keepdims=True) + epsilon) * gain
    return scaled.astype(jnp.bfloat16)


def window_attend(queries, keys_ext, values_ext, sink_rows, first_pos):
    row_count, head_count, head_size = queries.shape
    group_count = keys_ext.shape[1]
    span_rows = WINDOW // 2
    block_count = row_count // span_rows
    query_blocks = queries.reshape(
        block_count, span_rows, group_count, head_count // group_count, head_size
    )
    key_blocks = jnp.concatenate(
        [
            keys_ext[lag_index * span_rows : lag_index * span_rows + row_count].reshape(
                block_count, span_rows, group_count, head_size
            )
            for lag_index in range(3)
        ],
        axis=1,
    )
    value_blocks = jnp.concatenate(
        [
            values_ext[lag_index * span_rows : lag_index * span_rows + row_count].reshape(
                block_count, span_rows, group_count, head_size
            )
            for lag_index in range(3)
        ],
        axis=1,
    )
    scores = jnp.einsum(
        "nqgrd,nkgd->ngrqk", query_blocks, key_blocks, preferred_element_type=jnp.float32
    ) * head_size ** (-0.5)
    distance = WINDOW + jnp.arange(span_rows)[:, None] - jnp.arange(3 * span_rows)[None, :]
    key_pos = (
        first_pos
        - WINDOW
        + jnp.arange(block_count)[:, None] * span_rows
        + jnp.arange(3 * span_rows)[None, :]
    )
    is_valid = ((distance >= 0) & (distance < WINDOW))[None] & (key_pos >= 0)[:, None, :]
    is_valid = is_valid[:, None, None]
    sink_grid = sink_rows.reshape(1, group_count, head_count // group_count, 1)
    row_max = jnp.maximum(jnp.max(jnp.where(is_valid, scores, big_negative), axis=-1), sink_grid)
    weights = jnp.where(is_valid, jnp.exp(scores - row_max[..., None]), 0.0)
    row_total = jnp.sum(weights, axis=-1) + jnp.exp(sink_grid - row_max)
    prob_rows = (weights / row_total[..., None]).astype(jnp.bfloat16)
    mixed_sum = jnp.einsum(
        "ngrqk,nkgd->nqgrd", prob_rows, value_blocks, preferred_element_type=jnp.float32
    )
    return mixed_sum.reshape(row_count, head_count * head_size).astype(jnp.bfloat16)


def forget_groups(groups, keys, values, gates):
    head_count, head_size = (keys.shape[1], keys.shape[2])
    gates_all = lax.all_gather(gates, "sp", axis=0, tiled=True)

    def absorber(queries, query_gate, query_pos):

        def absorb(running, block):
            row_max, row_total, mixed_sum = running
            key_rows, value_rows, key_gate, key_pos = block
            scores = jnp.einsum(
                "qhd,khd->hqk", queries, key_rows, preferred_element_type=jnp.float32
            ) * head_size ** (-0.5)
            scores = scores + query_gate.T[:, :, None] - key_gate.T[:, None, :]
            is_valid = (query_pos[:, None] >= key_pos[None, :])[None]
            new_max = jnp.maximum(
                row_max, jnp.max(jnp.where(is_valid, scores, big_negative), axis=-1)
            )
            weights = jnp.where(is_valid, jnp.exp(scores - new_max[..., None]), 0.0)
            shrink = jnp.exp(row_max - new_max)
            row_total = row_total * shrink + jnp.sum(weights, axis=-1)
            mixed_sum = mixed_sum * shrink.T[:, :, None] + jnp.einsum(
                "hqk,khd->qhd",
                weights.astype(jnp.bfloat16),
                value_rows,
                preferred_element_type=jnp.float32,
            )
            return ((new_max, row_total, mixed_sum), None)

        return absorb

    initial = tuple(
        (
            (
                jnp.full((head_count, group[0].shape[0]), big_negative, jnp.float32),
                jnp.zeros((head_count, group[0].shape[0]), jnp.float32),
                jnp.zeros((group[0].shape[0], head_count, head_size), jnp.float32),
            )
            for group in groups
        )
    )
    first_row = jnp.int32(0)
    key_rows = lax.all_gather(keys, "sp", axis=0, tiled=True)
    value_rows = lax.all_gather(values, "sp", axis=0, tiled=True)
    piece_rows = key_rows.shape[0]
    sub_rows = math.gcd(piece_rows, 2048)
    turns = piece_rows // sub_rows
    key_gate = gates_all
    key_pos = jnp.arange(piece_rows)
    blocks = (
        key_rows.reshape(turns, sub_rows, head_count, head_size),
        value_rows.reshape(turns, sub_rows, head_count, head_size),
        key_gate.reshape(turns, sub_rows, head_count),
        key_pos.reshape(turns, sub_rows),
    )
    updated = []
    for (queries, query_gate, query_pos), state in zip(groups, initial):
        absorb = absorber(queries, query_gate, query_pos)

        def advance(current):
            return lax.scan(absorb, current, blocks)[0]

        def keep(current):
            return current

        updated.append(lax.cond(first_row <= query_pos[-1], advance, keep, state))
    finals = tuple(updated)
    return [
        (mixed_sum / row_total.T[:, :, None])
        .reshape(mixed_sum.shape[0], head_count * head_size)
        .astype(jnp.bfloat16)
        for row_max, row_total, mixed_sum in finals
    ]


def on_device(
    tokens,
    norm_gain,
    qk_gain,
    w_query_window,
    w_key_window,
    w_value_window,
    sink_logits,
    w_query_forget,
    w_key_forget,
    w_value_forget,
    gate_cum,
    w_merge,
    w_branch,
):
    row_count = tokens.shape[0]
    row_offset = lax.axis_index("sp") * row_count
    gathered = lax.all_gather(tokens, "tp", axis=1, tiled=True)
    as_float = gathered.astype(jnp.float32)
    normed = (
        as_float
        * lax.rsqrt(jnp.mean(as_float * as_float, axis=-1, keepdims=True) + epsilon)
        * norm_gain
    ).astype(jnp.bfloat16)
    merge_flat = w_merge.reshape(w_merge.shape[0], -1)
    pieces = (
        lax.all_gather(w_query_window, "sp", axis=0, tiled=True),
        lax.all_gather(w_key_window, "sp", axis=0, tiled=True),
        lax.all_gather(w_value_window, "sp", axis=0, tiled=True),
        lax.all_gather(w_query_forget, "sp", axis=0, tiled=True),
        lax.all_gather(w_key_forget, "sp", axis=0, tiled=True),
        lax.all_gather(w_value_forget, "sp", axis=0, tiled=True),
        lax.all_gather(merge_flat, "sp", axis=0, tiled=True),
    )
    projected = tuple(
        (jnp.dot(normed, weight_rows, preferred_element_type=jnp.float32) for weight_rows in pieces)
    )
    query_heads = w_query_window.shape[1] // HEAD
    group_heads = w_key_window.shape[1] // HEAD
    window_query = head_norm(projected[0], qk_gain[0], query_heads)
    window_key = head_norm(projected[1], qk_gain[1], group_heads)
    window_value = projected[2].astype(jnp.bfloat16).reshape(row_count, group_heads, HEAD)
    prev_key, prev_value = from_behind(
        (window_key[row_count - WINDOW :], window_value[row_count - WINDOW :]), "sp", 1
    )
    window_out = window_attend(
        window_query,
        jnp.concatenate([prev_key, window_key], axis=0),
        jnp.concatenate([prev_value, window_value], axis=0),
        sink_logits,
        row_offset,
    )
    forget_query = head_norm(projected[3], qk_gain[2], query_heads)
    forget_key = head_norm(projected[4], qk_gain[3], query_heads)
    forget_value = projected[5].astype(jnp.bfloat16).reshape(row_count, query_heads, HEAD)
    own_pos = row_offset + jnp.arange(row_count)
    forget_out = forget_groups(
        [(forget_query, gate_cum, own_pos)], forget_key, forget_value, gate_cum
    )[0]
    channel_count = w_merge.shape[2]
    merge_gate = jax.nn.sigmoid(projected[6]).reshape(row_count, 2, channel_count)
    branch_full = lax.all_gather(w_branch, "sp", axis=1, tiled=True)
    head_stack = jnp.stack([window_out, forget_out], axis=1)
    weight_rows = branch_full
    projection = jnp.einsum(
        "uxa,xag->uxg",
        lax.all_gather(head_stack, "tp", axis=2, tiled=True),
        weight_rows,
        preferred_element_type=jnp.float32,
    )
    return (merge_gate[:, 0] * projection[:, 0] + merge_gate[:, 1] * projection[:, 1]).astype(
        jnp.bfloat16
    )


def solution(mesh):
    return jax.shard_map(
        on_device,
        mesh=mesh,
        in_specs=(
            P(("grp", "sp"), "tp"),
            P(),
            P(),
            P("sp", "tp"),
            P("sp", "tp"),
            P("sp", "tp"),
            P("tp"),
            P("sp", "tp"),
            P("sp", "tp"),
            P("sp", "tp"),
            P(("grp", "sp"), "tp"),
            P("sp", None, "tp"),
            P(None, "sp", "tp"),
        ),
        out_specs=P(("grp", "sp"), "tp"),
        check_vma=False,
    )
```

profile of v0, /device:TPU:0, one launch (start us, length us, event | category | flops | bytes accessed | tf_op | source)
XLA Modules:
  0.0 339.6 jit_solution(14842164746860835694)
XLA Ops:
  11.2 1.3 slice.58
  13.7 16.6 %all_gather.48 = f32[1536,4]{0,1:T(4,128)} all-gather(f32[384,4]{0,1:T(4,128)} %param.27), channel_id=1, replica_groups=mesh['grp'=2,'sp'=4,'tp'=4] {'sp'}, dimensions={0}, use_global_device_ids=true | all-gather | bytes 30720 | tf_op jit(solution)/shard_map/all_gather | solution.py:76
  30.5 19.0 %all_gather.42 = bf16[2048,128]{1,0:T(8,128)(2,1)} all-gather(bf16[512,128]{1,0:T(8,128)(2,1)S(1)} %copy-done.8), channel_id=1, replica_groups=mesh['grp'=2,'sp'=4,'tp'=4] {'sp'}, dimensions={0}, use_global_device_ids=true | all-gather | bytes 655360 | tf_op jit(solution)/shard_map/all_gather | solution.py:175
  50.2 21.1 %all_gather.41 = bf16[2048,128]{1,0:T(8,128)(2,1)} all-gather(bf16[512,128]{1,0:T(8,128)(2,1)S(1)} %copy-done.9), channel_id=1, replica_groups=mesh['grp'=2,'sp'=4,'tp'=4] {'sp'}, dimensions={0}, use_global_device_ids=true | all-gather | bytes 655360 | tf_op jit(solution)/shard_map/all_gather | solution.py:176
  71.9 1.9 fusion.25
  74.3 2.5 multiply_reduce_fusion.1
  77.0 25.4 %all_gather.45 = bf16[1536,4,64]{0,2,1:T(8,128)(2,1)S(1)} all-gather(bf16[384,4,64]{0,2,1:T(8,128)(2,1)S(1)} %multiply_convert_fusion.2), channel_id=1, replica_groups=mesh['grp'=2,'sp'=4,'tp'=4] {'sp'}, dimensions={0}, use_global_device_ids=true | all-gather | bytes 983040 | tf_op jit(solution)/shard_map/all_gather | solution.py:115
  102.5 5.3 %all-gather.17.cloned.1.call-done = bf16[2048,256]{1,0:T(8,128)(2,1)} async-done(((bf16[512,256]{1,0:T(8,128)(2,1)}), bf16[2048,256]{1,0:T(8,128)(2,1)}) %all-gather.17.cloned.1.call-update) | async-done | bytes 1048592 | tf_op jit(solution)/shard_map/all_gather | solution.py:179
  107.7 2.0 convolution_convert_fusion.1
  109.7 25.2 %all_gather.47 = bf16[1536,4,64]{0,2,1:T(8,128)(2,1)S(1)} all-gather(bf16[384,4,64]{0,2,1:T(8,128)(2,1)S(1)} %bitcast.165), channel_id=1, replica_groups=mesh['grp'=2,'sp'=4,'tp'=4] {'sp'}, dimensions={0}, use_global_device_ids=true | all-gather | bytes 983040 | tf_op jit(solution)/shard_map/all_gather | solution.py:116
  134.9 8.7 %all-gather.19.cloned.1.call-done = bf16[2048,256]{1,0:T(8,128)(2,1)} async-done(((bf16[512,256]{1,0:T(8,128)(2,1)}), bf16[2048,256]{1,0:T(8,128)(2,1)}) %all-gather.19.cloned.1.call-update) | async-done | bytes 1048592 | tf_op jit(solution)/shard_map/all_gather | solution.py:177
  143.7 2.1 multiply_reduce_fusion
  145.7 1.2 multiply_reduce_fusion.2
  147.0 1.2 convolution_convert_fusion.2
  148.2 0.8 multiply_convert_fusion.1
  149.0 35.5 %conditional.1 = (f32[4,384]{1,0:T(4,128)}, f32[384,4,64]{0,2,1:T(8,128)}) conditional(s32[]{:T(128)} %bitcast.13, () %tuple.20, (bf16[1536,4,64]{0,2,1:T(8,128)(2,1)S(1)}, bf16[1536,4,64]{0,2,1:T(8,128)(2,1)S(1)}, f32[1536,4]{0,1:T(4,128)}, s32[3,512]{1,0:T(4,128)S(1)}, s32[3,512]{1,0:T(4,128)S(1)}, /*index=5*/s32[384]{0:T(512)}, ...), branch_computations={%region_7.8_spmd, %region_8.13_spmd} | conditional | flops 215199744 | bytes 15060769 | solution.py:138
  149.6 1.4 copy_bitcast_fusion
  151.0 33.5 %while.18 = (s32[]{:T(128)}, f32[4,384]{1,0:T(4,128)S(1)}, f32[4,384]{1,0:T(4,128)}, f32[384,4,64]{0,2,1:T(8,128)}, s32[384]{0:T(512)}, /*index=5*/s32[3,512]{1,...) while((s32[]{:T(128)}, f32[4,384]{1,0:T(4,128)S(1)}, ...), condition=%wide.region_12.12_spmd.clone, body=%wide.region_9.11_spmd.clone.sunk | while | flops 215196672 | bytes 11896481 | solution.py:133
  152.4 0.9 broadcast_compare_fusion.2
  153.2 2.7 fusion.85
  156.6 1.6 fusion.87
  158.8 2.7 fusion.89
  163.0 0.9 broadcast_compare_fusion.2
  163.8 2.7 fusion.85
  167.2 1.6 fusion.87
  168.8 1.3 fusion.88
  170.1 2.9 fusion.89
  174.4 0.9 broadcast_compare_fusion.2
  175.3 2.7 fusion.85
  178.7 1.6 fusion.87
  180.3 1.3 fusion.88
  181.6 2.9 fusion.89
  184.5 1.0 divide_convert_fusion.2
  185.5 2.5 bitcast_reduce_fusion
  189.8 2.8 collective-permute-start.1
  192.6 3.3 collective-permute-start
  195.9 1.0 multiply_convert_fusion
  200.0 1.0 fusion.32
  201.6 0.8 pad_maximum_fusion
  202.5 1.3 copy.55
  203.8 14.9 %all-gather.23.cloned.1.call-done = bf16[2,1024,512]{2,1,0:T(8,128)(2,1)} async-done(((bf16[2,256,512]{2,1,0:T(8,128)(2,1)}), bf16[2,1024,512]{2,1,0:T(8,128)(2,1)}) %all-gather.23.cloned.1.call-update) | async-done | bytes 2097168 | tf_op jit(solution)/shard_map/all_gather | solution.py:209
  218.6 21.5 %all-gather.21.cloned.1.call-done = bf16[384,2,1024]{2,0,1:T(8,128)(2,1)} async-done(((bf16[384,2,256]{2,0,1:T(8,128)(2,1)}), bf16[384,2,1024]{2,0,1:T(8,128)(2,1)}) %all-gather.21.cloned.1.call-update) | async-done | bytes 1572880 | tf_op jit(solution)/shard_map/all_gather | solution.py:214
  240.2 3.0 convolution_bitcast_fusion
  243.2 79.3 %all-gather.11.cloned.1.call-done = bf16[2048,1024]{1,0:T(8,128)(2,1)} async-done(((bf16[512,1024]{1,0:T(8,128)(2,1)}), bf16[2048,1024]{1,0:T(8,128)(2,1)}) %all-gather.11.cloned.1.call-update) | async-done | bytes 4194320 | tf_op jit(solution)/shard_map/all_gather | solution.py:180
  322.5 5.3 %add_divide_fusion = f32[384,1024]{1,0:T(8,128)} fusion(bf16[384,2048]{1,0:T(8,128)(2,1)S(1)} %copy-done.1, bf16[2048,1024]{1,0:T(8,128)(2,1)} %all-gather.11.cloned.1.call-done), kind=kOutput, calls=%fused_computation.44 | convolution fusion | flops 1611792384 | bytes 7340032 | tf_op jit(solution)/shard_map/dot_general | solution.py:183
  327.8 2.6 reshape.258
  330.5 1.2 fusion.56
  331.7 1.0 fusion.36
  (119 shorter events, 20.1 us)
Async XLA Ops:
  6.5 6.6 %copy-start.15 = (f32[4,64]{1,0:T(4,128)S(1)}, f32[4,64]{1,0:T(4,128)}, u32[]{:S(2)}) copy-start(f32[4,64]{1,0:T(4,128)} %param.19) | copy-start | bytes 3076
  6.5 24.0 %copy-start.8 = (bf16[512,128]{1,0:T(8,128)(2,1)S(1)}, bf16[512,128]{1,0:T(8,128)(2,1)}, u32[]{:S(2)}) copy-start(bf16[512,128]{1,0:T(8,128)(2,1)} %param.21) | copy-start | bytes 393220
  6.5 42.9 %copy-start.16 = (f32[4]{0:T(128)S(1)}, f32[4]{0:T(128)}, u32[]{:S(2)}) copy-start(f32[4]{0:T(128)} %param.23) | copy-start | bytes 52
  6.5 43.6 %copy-start.9 = (bf16[512,128]{1,0:T(8,128)(2,1)S(1)}, bf16[512,128]{1,0:T(8,128)(2,1)}, u32[]{:S(2)}) copy-start(bf16[512,128]{1,0:T(8,128)(2,1)} %param.22) | copy-start | bytes 393220
  6.5 65.4 %all-gather.9.cloned.1.call-start = ((), (), s32[]{:S(2)}) async-start(), calls=%async_computation | async-start | bytes 1966080 | tf_op jit(solution)/shard_map/all_gather | solution.py:165
  7.3 67.1 %all-gather.15.cloned.1.call-start = ((), (), s32[]{:S(2)}) async-start(), calls=%async_computation.3 | async-start | bytes 1310720 | tf_op jit(solution)/shard_map/all_gather | solution.py:178
  8.0 99.7 %all-gather.17.cloned.1.call-start = ((), (), s32[]{:S(2)}) async-start(), calls=%async_computation.4 | async-start | bytes 1310720 | tf_op jit(solution)/shard_map/all_gather | solution.py:179
  8.8 134.9 %all-gather.19.cloned.1.call-start = ((), (), s32[]{:S(2)}) async-start(), calls=%async_computation.5 | async-start | bytes 1310720 | tf_op jit(solution)/shard_map/all_gather | solution.py:177
  9.3 176.2 %all-gather.13.cloned.1.call-start = ((), (), s32[]{:S(2)}) async-start(), calls=%async_computation.2 | async-start | bytes 1310720 | tf_op jit(solution)/shard_map/all_gather | solution.py:174
  9.9 208.7 %all-gather.23.cloned.1.call-start = ((), (), s32[]{:S(2)}) async-start(), calls=%async_computation.7 | async-start | bytes 2621440 | tf_op jit(solution)/shard_map/all_gather | solution.py:209
  10.5 63.4 %copy-start.11 = (f32[2048]{0:T(1024)S(1)}, f32[2048]{0:T(1024)}, u32[]{:S(2)}) copy-start(f32[2048]{0:T(1024)} %param.18) | copy-start | bytes 24580
  10.5 229.6 %all-gather.21.cloned.1.call-start = ((), (), s32[]{:S(2)}) async-start(), calls=%async_computation.6 | async-start | bytes 1966080 | tf_op jit(solution)/shard_map/all_gather | solution.py:214
  71.9 1.9 copy-start.2
  74.3 72.6 %copy-start = (bf16[384,2048]{1,0:T(8,128)(2,1)}, bf16[384,2048]{1,0:T(8,128)(2,1)S(1)}, u32[]{:S(2)}) copy-start(bf16[384,2048]{1,0:T(8,128)(2,1)S(1)} %fusion.27) | copy-start | bytes 4718596
  143.7 2.1 copy-start.3
  145.7 1.2 copy-start.4
  185.5 2.6 copy-start.5
  188.4 1.1 copy-start.10
  188.4 1.2 copy-start.12
  188.6 7.3 %copy-start.14 = (f32[64]{0:T(128)S(1)}, f32[64]{0:T(128)}, u32[]{:S(2)}) copy-start(f32[64]{0:T(128)} %get-tuple-element.195) | copy-start | bytes 772
  189.8 7.2 %collective-permute-start.1 = (bf16[128,2,64]{0,2,1:T(8,128)(2,1)S(1)}, bf16[128,2,64]{0,2,1:T(8,128)(2,1)S(1)}, u32[]{:S(2)}, u32[]{:S(2)}) collective-permute-start(bf16[128,2,64]{0,2,1:T(8,128)(2,1)S(1)} %slice.68), channel_id=1, source_target_pairs={{0,4},{4,8},{8,12},{1,5},{5,9},{9,13},{2,6},{6,10},{10,14},{3,7},{... | collective-permute-start | bytes 98312 | tf_op jit(solution)/shard_map/ppermute | solution.py:16
  192.6 5.4 %collective-permute-start = (bf16[128,2,64]{0,2,1:T(8,128)(2,1)S(1)}, bf16[128,2,64]{0,2,1:T(8,128)(2,1)S(1)}, u32[]{:S(2)}, u32[]{:S(2)}) collective-permute-start(bf16[128,2,64]{0,2,1:T(8,128)(2,1)S(1)} %bitcast.167), channel_id=1, source_target_pairs={{0,4},{4,8},{8,12},{1,5},{5,9},{9,13},{2,6},{6,10},{10,14},{3,7},{... | collective-permute-start | bytes 98312 | tf_op jit(solution)/shard_map/ppermute | solution.py:16
  197.3 1.2 copy-start.7
  198.5 0.7 copy-start.13
  200.9 1.5 copy-start.6
  202.4 120.1 %all-gather.11.cloned.1.call-start = ((), (), s32[]{:S(2)}) async-start(), calls=%async_computation.1 | async-start | bytes 5242880 | tf_op jit(solution)/shard_map/all_gather | solution.py:180
  203.8 118.7 %copy-start.1 = (bf16[384,2048]{1,0:T(8,128)(2,1)S(1)}, bf16[384,2048]{1,0:T(8,128)(2,1)}, u32[]{:S(2)}) copy-start(bf16[384,2048]{1,0:T(8,128)(2,1)} %copy-done) | copy-start | bytes 4718596
Sparse Core Ops, SparseCore 0:
  8.9 22.3 all-gather.8
  32.9 36.9 all-gather.14
  71.5 36.1 all-gather.16
  109.1 34.4 all-gather.18
  145.1 27.0 all-gather.12
  173.6 45.0 all-gather.22
  220.2 19.9 all-gather.20
  241.7 80.7 all-gather.10
where the time goes:
time: 341 us; the launch traced here: 340 us
  waiting for transfers between devices  134 us (39%)
  blocking collectives  107 us (31%)
  matrix products  37.9 us (11%)
  other arithmetic  23.1 us (7%)
  local copies, waits for them, and re-layouts  16.3 us (5%)
  between operations  14.7 us (4%)
  starting transfers between devices  6.38 us (2%)
    all_gather x1, waiting for transfers between devices, on_device(): lax.all_gather(merge_flat, 'sp', axis=0, tiled=True)  79.3 us
    all_gather x1, blocking collectives, forget_groups(): key_rows = lax.all_gather(keys, 'sp', axis=0, tiled=True)  25.4 us
    all_gather x1, blocking collectives, forget_groups(): value_rows = lax.all_gather(values, 'sp', axis=0, tiled=True)  25.2 us
    all_gather x1, waiting for transfers between devices, on_device(): lax.all_gather(head_stack, 'tp', axis=2, tiled=True)  21.5 us
    all_gather x1, blocking collectives, on_device(): lax.all_gather(w_value_window, 'sp', axis=0, tiled=True)  21.1 us
    all_gather x1, blocking collectives, on_device(): lax.all_gather(w_key_window, 'sp', axis=0, tiled=True)  19 us
    dot_general x7, matrix products, on_device(): jnp.dot(normed, weight_rows, preferred_element_type=jnp.float32)  16.8 us
    all_gather x1, blocking collectives, forget_groups(): gates_all = lax.all_gather(gates, 'sp', axis=0, tiled=True)  16.6 us
  transfers between devices with their start and end apart: 10, of which 6 were waited for; matrix products, arithmetic and copies ran while one was open for 20% of the time, Pallas kernels for 0%

commit v1 on v0

--- a/solution.py
+++ b/solution.py
@@ -8,6 +8,22 @@
 WINDOW = 128
 epsilon = 1e-06
 big_negative = -1e30
+
+
+def ring_product(shard, axis, dim, term):
+    peers, place, extent = (lax.axis_size(axis), lax.axis_index(axis), shard.shape[dim])
+    right = [(i, (i + 1) % peers) for i in range(peers)]
+    left = [(i, (i - 1) % peers) for i in range(peers)]
+    half = peers // 2
+    from_left = from_right = shard
+    so_far = term(shard, place * extent)
+    for turn in range(1, half + 1):
+        from_left = lax.ppermute(from_left, axis, right)
+        if turn < peers - half:
+            from_right = lax.ppermute(from_right, axis, left)
+            so_far = so_far + term(from_right, (place + turn) % peers * extent)
+        so_far = so_far + term(from_left, (place - turn) % peers * extent)
+    return so_far
 
 
 def from_behind(value, axis, by):
@@ -209,11 +225,16 @@
     branch_full = lax.all_gather(w_branch, "sp", axis=1, tiled=True)
     head_stack = jnp.stack([window_out, forget_out], axis=1)
     weight_rows = branch_full
-    projection = jnp.einsum(
-        "uxa,xag->uxg",
-        lax.all_gather(head_stack, "tp", axis=2, tiled=True),
-        weight_rows,
-        preferred_element_type=jnp.float32,
+    projection = ring_product(
+        head_stack,
+        "tp",
+        2,
+        lambda shard, at: jnp.einsum(
+            "uxa,xag->uxg",
+            shard,
+            lax.dynamic_slice_in_dim(weight_rows, at, shard.shape[2], axis=1),
+            preferred_element_type=jnp.float32,
+        ),
     )
     return (merge_gate[:, 0] * projection[:, 0] + merge_gate[:, 1] * projection[:, 1]).astype(
         jnp.bfloat16

time: 341 us -> 317 us (0.930)
  waiting for transfers between devices: 134 us -> 102 us
  local copies, waits for them, and re-layouts: 16.3 us -> 21.9 us
    all_gather x1 -> x0, waiting for transfers between devices: 21.5 us -> none  [on_device(): lax.all_gather(head_stack, 'tp', axis=2, tiled=True)]
    all_gather x1, waiting for transfers between devices: 79.3 us -> 58 us  [on_device(): lax.all_gather(merge_flat, 'sp', axis=0, tiled=True)]
    all_gather x1, waiting for transfers between devices: 5.25 us -> 23.9 us  [on_device(): lax.all_gather(w_value_forget, 'sp', axis=0, tiled=True)]
    all_gather x1, waiting for transfers between devices: 14.9 us -> 0.01 us  [on_device(): branch_full = lax.all_gather(w_branch, 'sp', axis=1, tiled=True)]
    ppermute x0 -> x3, waiting for transfers between devices: none -> 12.4 us  [the longest x2 12.4 us: ring_product(): from_left = lax.ppermute(from_left, axis, right)]
    all_gather x1, waiting for transfers between devices: 8.71 us -> 4 us  [on_device(): lax.all_gather(w_query_forget, 'sp', axis=0, tiled=True)]
  transfers between devices with their start and end apart: 10 -> 12, of which waited for: 6 -> 5; matrix products, arithmetic and copies ran while one was open for 20% -> 24% of each run, Pallas kernels for 0% -> 0%
where the time goes in v1:
time: 317 us; the launch traced here: 316 us
  blocking collectives  107 us (34%)
  waiting for transfers between devices  102 us (32%)
  matrix products  38.4 us (12%)
  other arithmetic  23.7 us (7%)
  local copies, waits for them, and re-layouts  21.9 us (7%)
  between operations  14.7 us (5%)
  starting transfers between devices  8.58 us (3%)
    all_gather x1, waiting for transfers between devices, on_device(): lax.all_gather(merge_flat, 'sp', axis=0, tiled=True)  58 us
    all_gather x1, blocking collectives, forget_groups(): key_rows = lax.all_gather(keys, 'sp', axis=0, tiled=True)  26.3 us
    all_gather x1, blocking collectives, forget_groups(): value_rows = lax.all_gather(values, 'sp', axis=0, tiled=True)  24.5 us
    all_gather x1, waiting for transfers between devices, on_device(): lax.all_gather(w_value_forget, 'sp', axis=0, tiled=True)  23.9 us
    all_gather x1, blocking collectives, on_device(): lax.all_gather(w_value_window, 'sp', axis=0, tiled=True)  20.1 us
    all_gather x1, blocking collectives, on_device(): lax.all_gather(w_key_window, 'sp', axis=0, tiled=True)  19.3 us
    all_gather x1, blocking collectives, forget_groups(): gates_all = lax.all_gather(gates, 'sp', axis=0, tiled=True)  16.6 us
    dot_general x7, matrix products, on_device(): jnp.dot(normed, weight_rows, preferred_element_type=jnp.float32)  15.4 us
  transfers between devices with their start and end apart: 12, of which 5 were waited for; matrix products, arithmetic and copies ran while one was open for 24% of the time, Pallas kernels for 0%

profile of v1, /device:TPU:0, one launch (start us, length us, event | category | flops | bytes accessed | tf_op | source)
XLA Modules:
  0.0 315.7 jit_solution(14214364911437549301)
XLA Ops:
  10.0 1.0 copy.31
  11.1 1.3 copy.58
  13.1 1.3 slice.58
  15.6 16.6 %all_gather.46 = f32[1536,4]{0,1:T(4,128)} all-gather(f32[384,4]{0,1:T(4,128)} %param.27), channel_id=1, replica_groups=mesh['grp'=2,'sp'=4,'tp'=4] {'sp'}, dimensions={0}, use_global_device_ids=true | all-gather | bytes 30720 | tf_op jit(solution)/shard_map/all_gather | solution.py:92
  32.4 19.3 %all_gather.40 = bf16[2048,128]{1,0:T(8,128)(2,1)} all-gather(bf16[512,128]{1,0:T(8,128)(2,1)S(1)} %copy-done.9), channel_id=1, replica_groups=mesh['grp'=2,'sp'=4,'tp'=4] {'sp'}, dimensions={0}, use_global_device_ids=true | all-gather | bytes 655360 | tf_op jit(solution)/shard_map/all_gather | solution.py:191
  52.4 20.1 %all_gather.39 = bf16[2048,128]{1,0:T(8,128)(2,1)S(1)} all-gather(bf16[512,128]{1,0:T(8,128)(2,1)S(1)} %copy-done.10), channel_id=1, replica_groups=mesh['grp'=2,'sp'=4,'tp'=4] {'sp'}, dimensions={0}, use_global_device_ids=true | all-gather | bytes 655360 | tf_op jit(solution)/shard_map/all_gather | solution.py:192
  72.6 1.9 fusion.25
  75.0 2.5 multiply_reduce_fusion.1
  77.6 26.3 %all_gather.43 = bf16[1536,4,64]{0,2,1:T(8,128)(2,1)S(1)} all-gather(bf16[384,4,64]{0,2,1:T(8,128)(2,1)S(1)} %multiply_convert_fusion.2), channel_id=1, replica_groups=mesh['grp'=2,'sp'=4,'tp'=4] {'sp'}, dimensions={0}, use_global_device_ids=true | all-gather | bytes 983040 | tf_op jit(solution)/shard_map/all_gather | solution.py:131
  103.9 4.0 %all-gather.20.cloned.1.call-done = bf16[2048,256]{1,0:T(8,128)(2,1)} async-done(((bf16[512,256]{1,0:T(8,128)(2,1)}), bf16[2048,256]{1,0:T(8,128)(2,1)}) %all-gather.20.cloned.1.call-update) | async-done | bytes 1048592 | tf_op jit(solution)/shard_map/all_gather | solution.py:193
  107.9 2.0 multiply_reduce_fusion
  112.8 23.9 %all-gather.18.cloned.1.call-done = bf16[2048,256]{1,0:T(8,128)(2,1)} async-done(((bf16[512,256]{1,0:T(8,128)(2,1)}), bf16[2048,256]{1,0:T(8,128)(2,1)}) %all-gather.18.cloned.1.call-update) | async-done | bytes 1048592 | tf_op jit(solution)/shard_map/all_gather | solution.py:195
  136.6 2.0 convolution_convert_fusion.1
  138.6 24.5 %all_gather.45 = bf16[1536,4,64]{0,2,1:T(8,128)(2,1)S(1)} all-gather(bf16[384,4,64]{0,2,1:T(8,128)(2,1)S(1)} %bitcast.168), channel_id=1, replica_groups=mesh['grp'=2,'sp'=4,'tp'=4] {'sp'}, dimensions={0}, use_global_device_ids=true | all-gather | bytes 983040 | tf_op jit(solution)/shard_map/all_gather | solution.py:132
  163.1 35.5 %conditional.1 = (f32[4,384]{1,0:T(4,128)}, f32[384,4,64]{0,2,1:T(8,128)}) conditional(s32[]{:T(128)} %bitcast.13, () %tuple.20, (bf16[1536,4,64]{0,2,1:T(8,128)(2,1)S(1)}, bf16[1536,4,64]{0,2,1:T(8,128)(2,1)S(1)}, f32[1536,4]{0,1:T(4,128)}, s32[3,512]{1,0:T(4,128)S(1)}, s32[3,512]{1,0:T(4,128)S(1)}, /*index=5*/s32[384]{0:T(512)}, ...), branch_computations={%region_7.8_spmd, %region_8.13_spmd} | conditional | flops 215199744 | bytes 15060769 | solution.py:154
  163.8 1.3 copy_bitcast_fusion
  165.1 33.5 %while.18 = (s32[]{:T(128)}, f32[4,384]{1,0:T(4,128)S(1)}, f32[4,384]{1,0:T(4,128)}, f32[384,4,64]{0,2,1:T(8,128)}, s32[384]{0:T(512)}, /*index=5*/s32[3,512]{1,...) while((s32[]{:T(128)}, f32[4,384]{1,0:T(4,128)S(1)}, ...), condition=%wide.region_12.12_spmd.clone, body=%wide.region_9.11_spmd.clone.sunk | while | flops 215196672 | bytes 11896481 | solution.py:149
  167.3 2.7 fusion.96
  170.7 1.6 fusion.98
  173.0 2.7 fusion.100
  178.0 2.7 fusion.96
  181.3 1.6 fusion.98
  183.0 1.3 fusion.99
  184.3 2.9 fusion.100
  189.4 2.7 fusion.96
  192.8 1.6 fusion.98
  194.4 1.3 fusion.99
  195.7 2.9 fusion.100
  198.6 1.0 divide_convert_fusion.2
  199.8 2.5 bitcast_reduce_fusion
  203.2 1.5 reshape.266
  204.8 1.0 copy.42
  206.7 3.6 %collective-permute-start.1 = (bf16[128,2,64]{0,2,1:T(8,128)(2,1)S(1)}, bf16[128,2,64]{0,2,1:T(8,128)(2,1)S(1)}, u32[]{:S(2)}, u32[]{:S(2)}) collective-permute-start(bf16[128,2,64]{0,2,1:T(8,128)(2,1)S(1)} %slice.68), channel_id=1, source_target_pairs={{0,4},{4,8},{8,12},{1,5},{5,9},{9,13},{2,6},{6,10},{10,14},{3,7},{... | collective-permute-start | bytes 98312 | tf_op jit(solution)/shard_map/ppermute | solution.py:32
  210.2 1.0 copy.35
  211.2 2.9 collective-permute-start
  214.2 2.6 multiply_convert_fusion
  216.7 1.5 fusion.53
  220.0 1.5 fusion.28
  222.4 0.9 fusion.32
  224.2 1.7 collective-permute-start.2
  225.9 7.9 %collective-permute-done.3 = bf16[384,2,256]{2,0,1:T(8,128)(2,1)S(1)} collective-permute-done((bf16[384,2,256]{2,0,1:T(8,128)(2,1)S(1)}, bf16[384,2,256]{2,0,1:T(8,128)(2,1)S(1)}, u32[]{:S(2)}, u32[]{:S(2)}) %collective-permute-start.3) | collective-permute-done | bytes 393248 | tf_op jit(solution)/shard_map/ppermute | solution.py:21
  233.9 1.6 fusion.37
  236.6 4.5 %collective-permute-done.4 = bf16[384,2,256]{2,0,1:T(8,128)(2,1)} collective-permute-done((bf16[384,2,256]{2,0,1:T(8,128)(2,1)S(1)}, bf16[384,2,256]{2,0,1:T(8,128)(2,1)}, u32[]{:S(2)}, u32[]{:S(2)}) %collective-permute-start.4) | collective-permute-done | bytes 393248 | tf_op jit(solution)/shard_map/ppermute | solution.py:21
  241.1 1.5 add_bitcast_fusion
  242.5 58.0 %all-gather.10.cloned.1.call-done = bf16[2048,1024]{1,0:T(8,128)(2,1)} async-done(((bf16[512,1024]{1,0:T(8,128)(2,1)}), bf16[2048,1024]{1,0:T(8,128)(2,1)}) %all-gather.10.cloned.1.call-update) | async-done | bytes 4194320 | tf_op jit(solution)/shard_map/all_gather | solution.py:196
  300.6 5.3 %add_divide_fusion = f32[384,1024]{1,0:T(8,128)} fusion(bf16[384,2048]{1,0:T(8,128)(2,1)S(1)} %copy-done.1, bf16[2048,1024]{1,0:T(8,128)(2,1)} %all-gather.10.cloned.1.call-done), kind=kOutput, calls=%fused_computation.45 | convolution fusion | flops 1611792384 | bytes 7340032 | tf_op jit(solution)/shard_map/dot_general | solution.py:199
  305.9 1.9 copy.55
  307.9 0.9 copy.47
  (124 shorter events, 25.8 us)
Async XLA Ops:
  6.5 3.4 %copy-start.6 = (bf16[2,256,512]{2,1,0:T(8,128)(2,1)S(1)}, bf16[2,256,512]{2,1,0:T(8,128)(2,1)}, u32[]{:S(2)}) copy-start(bf16[2,256,512]{2,1,0:T(8,128)(2,1)} %param.29) | copy-start | bytes 1572868
  6.5 4.5 %copy-start.5 = (bf16[512,2,512]{2,1,0:T(2,128)(2,1)S(1)}, bf16[512,2,512]{2,1,0:T(2,128)(2,1)}, u32[]{:S(2)}) copy-start(bf16[512,2,512]{2,1,0:T(2,128)(2,1)} %param.28) | copy-start | bytes 3145732
  6.5 66.0 %all-gather.8.cloned.1.call-start = ((), (), s32[]{:S(2)}) async-start(), calls=%async_computation | async-start | bytes 1966080 | tf_op jit(solution)/shard_map/all_gather | solution.py:181
  7.3 67.7 %all-gather.16.cloned.1.call-start = ((), (), s32[]{:S(2)}) async-start(), calls=%async_computation.4 | async-start | bytes 1310720 | tf_op jit(solution)/shard_map/all_gather | solution.py:194
  8.0 99.9 %all-gather.20.cloned.1.call-start = ((), (), s32[]{:S(2)}) async-start(), calls=%async_computation.6 | async-start | bytes 1310720 | tf_op jit(solution)/shard_map/all_gather | solution.py:193
  8.7 127.9 %all-gather.18.cloned.1.call-start = ((), (), s32[]{:S(2)}) async-start(), calls=%async_computation.5 | async-start | bytes 1310720 | tf_op jit(solution)/shard_map/all_gather | solution.py:195
  9.3 190.5 %all-gather.14.cloned.1.call-start = ((), (), s32[]{:S(2)}) async-start(), calls=%async_computation.3 | async-start | bytes 1310720 | tf_op jit(solution)/shard_map/all_gather | solution.py:190
  9.9 224.0 %all-gather.12.cloned.1.call-start = ((), (), s32[]{:S(2)}) async-start(), calls=%async_computation.2 | async-start | bytes 2621440 | tf_op jit(solution)/shard_map/all_gather | solution.py:225
  11.0 289.6 %all-gather.10.cloned.1.call-start = ((), (), s32[]{:S(2)}) async-start(), calls=%async_computation.1 | async-start | bytes 5242880 | tf_op jit(solution)/shard_map/all_gather | solution.py:196
  11.0 3.9 %copy-start.14 = (f32[4,64]{1,0:T(4,128)S(1)}, f32[4,64]{1,0:T(4,128)}, u32[]{:S(2)}) copy-start(f32[4,64]{1,0:T(4,128)} %param.19) | copy-start | bytes 3076
  11.1 21.3 %copy-start.9 = (bf16[512,128]{1,0:T(8,128)(2,1)S(1)}, bf16[512,128]{1,0:T(8,128)(2,1)}, u32[]{:S(2)}) copy-start(bf16[512,128]{1,0:T(8,128)(2,1)} %param.21) | copy-start | bytes 393220
  11.1 40.6 %copy-start.15 = (f32[4]{0:T(128)S(1)}, f32[4]{0:T(128)}, u32[]{:S(2)}) copy-start(f32[4]{0:T(128)} %param.23) | copy-start | bytes 52
  11.1 41.3 %copy-start.10 = (bf16[512,128]{1,0:T(8,128)(2,1)S(1)}, bf16[512,128]{1,0:T(8,128)(2,1)}, u32[]{:S(2)}) copy-start(bf16[512,128]{1,0:T(8,128)(2,1)} %param.22) | copy-start | bytes 393220
  12.4 62.0 %copy-start.11 = (f32[2048]{0:T(1024)S(1)}, f32[2048]{0:T(1024)}, u32[]{:S(2)}) copy-start(f32[2048]{0:T(1024)} %param.18) | copy-start | bytes 24580
  72.5 1.9 copy-start.2
  74.9 61.7 %copy-start = (bf16[384,2048]{1,0:T(8,128)(2,1)}, bf16[384,2048]{1,0:T(8,128)(2,1)S(1)}, u32[]{:S(2)}) copy-start(bf16[384,2048]{1,0:T(8,128)(2,1)S(1)} %fusion.27) | copy-start | bytes 4718596
  202.3 3.5 %copy-start.1 = (bf16[384,2048]{1,0:T(8,128)(2,1)S(1)}, bf16[384,2048]{1,0:T(8,128)(2,1)}, u32[]{:S(2)}) copy-start(bf16[384,2048]{1,0:T(8,128)(2,1)} %copy-done) | copy-start | bytes 4718596
  202.3 3.4 %copy-start.3 = (bf16[2048,128]{1,0:T(8,128)(2,1)S(1)}, bf16[2048,128]{1,0:T(8,128)(2,1)}, u32[]{:S(2)}) copy-start(bf16[2048,128]{1,0:T(8,128)(2,1)} %all_gather.40) | copy-start | bytes 1572868
  205.8 0.8 copy-start.12
  206.7 11.5 %collective-permute-start.1 = (bf16[128,2,64]{0,2,1:T(8,128)(2,1)S(1)}, bf16[128,2,64]{0,2,1:T(8,128)(2,1)S(1)}, u32[]{:S(2)}, u32[]{:S(2)}) collective-permute-start(bf16[128,2,64]{0,2,1:T(8,128)(2,1)S(1)} %slice.68), channel_id=1, source_target_pairs={{0,4},{4,8},{8,12},{1,5},{5,9},{9,13},{2,6},{6,10},{10,14},{3,7},{... | collective-permute-start | bytes 98312 | tf_op jit(solution)/shard_map/ppermute | solution.py:32
  211.2 7.5 %collective-permute-start = (bf16[128,2,64]{0,2,1:T(8,128)(2,1)}, bf16[128,2,64]{0,2,1:T(8,128)(2,1)S(1)}, u32[]{:S(2)}, u32[]{:S(2)}) collective-permute-start(bf16[128,2,64]{0,2,1:T(8,128)(2,1)} %bitcast.170), channel_id=1, source_target_pairs={{0,4},{4,8},{8,12},{1,5},{5,9},{9,13},{2,6},{6,10},{10,14},{3,7},{... | collective-permute-start | bytes 98312 | tf_op jit(solution)/shard_map/ppermute | solution.py:32
  218.5 1.5 copy-start.7
  220.0 1.5 copy-start.13
  221.5 0.9 copy-start.8
  224.1 9.7 %collective-permute-start.3 = (bf16[384,2,256]{2,0,1:T(8,128)(2,1)S(1)}, bf16[384,2,256]{2,0,1:T(8,128)(2,1)S(1)}, u32[]{:S(2)}, u32[]{:S(2)}) collective-permute-start(bf16[384,2,256]{2,0,1:T(8,128)(2,1)S(1)} %pad_maximum_fusion), channel_id=1, source_target_pairs={{0,1},{1,2},{2,3},{3,0},{4,5},{5,6},{6,7},{7,4},{8,9},{9,10},{10,1... | collective-permute-start | bytes 1179656 | tf_op jit(solution)/shard_map/ppermute | solution.py:21
  224.2 11.9 %collective-permute-start.2 = (bf16[384,2,256]{2,0,1:T(8,128)(2,1)S(1)}, bf16[384,2,256]{2,0,1:T(8,128)(2,1)S(1)}, u32[]{:S(2)}, u32[]{:S(2)}) collective-permute-start(bf16[384,2,256]{2,0,1:T(8,128)(2,1)S(1)} %pad_maximum_fusion), channel_id=1, source_target_pairs={{0,3},{1,0},{2,1},{3,2},{4,7},{5,4},{6,5},{7,6},{8,11},{9,8},{10,9... | collective-permute-start | bytes 1179656 | tf_op jit(solution)/shard_map/ppermute | solution.py:23
  233.8 7.3 %collective-permute-start.4 = (bf16[384,2,256]{2,0,1:T(8,128)(2,1)S(1)}, bf16[384,2,256]{2,0,1:T(8,128)(2,1)}, u32[]{:S(2)}, u32[]{:S(2)}) collective-permute-start(bf16[384,2,256]{2,0,1:T(8,128)(2,1)S(1)} %collective-permute-done.3), channel_id=1, source_target_pairs={{0,1},{1,2},{2,3},{3,0},{4,5},{5,6},{6,7},{7,4},{8,9},{9,10},{10,1... | collective-permute-start | bytes 1179656 | tf_op jit(solution)/shard_map/ppermute | solution.py:21
  233.9 1.8 copy-start.4
Sparse Core Ops, SparseCore 0:
  8.9 22.3 all-gather.7
  32.8 37.7 all-gather.15
  72.3 35.5 all-gather.19
  109.3 27.2 all-gather.17
  138.1 34.2 all-gather.13
  173.7 45.2 all-gather.11
  220.7 79.8 all-gather.9
